TPU v7x, 32 devices: a whole 2x2x4 slice. The times are simulated.
32 devices in a mesh: fs: 8 (over z, y), tp: 4 (over x, core).
Axes of the slice: x: 2, y: 2, z: 4, core: 2. Of those that a mesh axis runs over, the one named last changes fastest.
Arguments:
- tokens: bfloat16 [8, 384, 2048], P('fs', None, 'tp'), may hold values from -16 to 16
- first_gate: bfloat16 [2048, 6144], P('fs', 'tp'), may hold values from -0.125 to 0.125
- first_up: bfloat16 [2048, 6144], P('fs', 'tp'), may hold values from -0.125 to 0.125
- first_down: bfloat16 [6144, 2048], P('tp', 'fs'), may hold values from -0.078125 to 0.078125
- first_gain: bfloat16 [2048], P('tp'), may hold values from 0.099609375 to 1.8984375
- glu_value: bfloat16 [2048, 1024], P('fs', 'tp'), may hold values from -0.125 to 0.125
- glu_gate: bfloat16 [2048, 1024], P('fs', 'tp'), may hold values from -0.125 to 0.125
- conv_taps: bfloat16 [31, 1024], P(None, 'tp'), may hold values from -3 to 3
- conv_gain: bfloat16 [1024], P('tp'), may hold values from 0.099609375 to 1.8984375
- conv_proj: bfloat16 [1024, 2048], P('tp', 'fs'), may hold values from -0.1875 to 0.1875
- second_gain: bfloat16 [2048], P('tp'), may hold values from 0.099609375 to 1.8984375
- last_gate: bfloat16 [2048, 6144], P('fs', 'tp'), may hold values from -0.125 to 0.125
- last_up: bfloat16 [2048, 6144], P('fs', 'tp'), may hold values from -0.125 to 0.125
- last_down: bfloat16 [6144, 2048], P('tp', 'fs'), may hold values from -0.078125 to 0.078125
- third_gain: bfloat16 [2048], P('tp'), may hold values from 0.099609375 to 1.8984375
Outputs:
- layer_out: bfloat16 [8, 384, 2048], P('fs', None, 'tp')
All inputs are finite; a program needn't handle non-finite values.
Results may differ from a plain program's by a relative error of at most 0.015.
Values may be sent and summed in bfloat16 or wider, within the bound.
A program may use at most 64 MiB of HBM per device.

v0:
```python
import jax
import jax.numpy as jnp
from jax import lax
from jax.sharding import PartitionSpec as P

ALPHA = 2.0**0.25
EPSILON = 1e-05


def norm_split(values, gain):
    width_all = values.shape[-1] * lax.axis_size("tp")
    sums, squares = lax.psum(
        (jnp.sum(values, axis=-1, keepdims=True), jnp.sum(values * values, axis=-1, keepdims=True)),
        "tp",
    )
    center = sums / width_all
    spread = squares / width_all - center * center
    return (values - center) * lax.rsqrt(spread + EPSILON) * gain.astype(jnp.float32)


def gather_features(current):
    return lax.all_gather(current, "tp", axis=1, tiled=True)


def scatter_rows(partial_value):
    return lax.psum_scatter(
        partial_value.astype(jnp.bfloat16), "tp", scatter_dimension=1, tiled=True
    ).astype(jnp.float32)


def fold_rows(gathered, shard_rows):
    return (
        jnp.dot(gathered, shard_rows[0], preferred_element_type=jnp.float32),
        jnp.dot(gathered, shard_rows[1], preferred_element_type=jnp.float32),
    )


def feed_forward(current, w_gate, w_up, w_down):
    gathered = gather_features(current)
    gate, upward = fold_rows(
        gathered,
        (
            lax.all_gather(w_gate, "fs", axis=0, tiled=True),
            lax.all_gather(w_up, "fs", axis=0, tiled=True),
        ),
    )
    hidden = (jax.nn.silu(gate) * upward).astype(jnp.bfloat16)
    partial_value = jnp.dot(
        hidden, lax.all_gather(w_down, "fs", axis=1, tiled=True), preferred_element_type=jnp.float32
    )
    return scatter_rows(partial_value)


def conv_module(current, glu_value, glu_gate, conv_taps, conv_gain, conv_proj):
    gathered = gather_features(current)
    value, gate = fold_rows(
        gathered,
        (
            lax.all_gather(glu_value, "fs", axis=0, tiled=True),
            lax.all_gather(glu_gate, "fs", axis=0, tiled=True),
        ),
    )
    gated = value * jax.nn.sigmoid(gate)
    reach = (conv_taps.shape[0] - 1) // 2
    length = gated.shape[0]
    padded = jnp.pad(gated, ((reach, reach), (0, 0)))
    taps = conv_taps.astype(jnp.float32)
    mixed = jnp.zeros_like(gated)
    for tap_index in range(conv_taps.shape[0]):
        mixed = mixed + taps[tap_index] * padded[tap_index : tap_index + length]
    normed = jax.nn.silu(norm_split(mixed, conv_gain)).astype(jnp.bfloat16)
    partial_value = jnp.dot(
        normed,
        lax.all_gather(conv_proj, "fs", axis=1, tiled=True),
        preferred_element_type=jnp.float32,
    )
    return scatter_rows(partial_value)


def post_norm(current, branch, weight, gain):
    mixed = ALPHA * current.astype(jnp.float32) + weight * branch
    return norm_split(mixed, gain).astype(jnp.bfloat16)


def body(
    tokens,
    first_gate,
    first_up,
    first_down,
    first_gain,
    glu_value,
    glu_gate,
    conv_taps,
    conv_gain,
    conv_proj,
    second_gain,
    last_gate,
    last_up,
    last_down,
    third_gain,
):
    current = tokens[0]
    first = post_norm(
        current, feed_forward(current, first_gate, first_up, first_down), 0.5, first_gain
    )
    second = post_norm(
        first,
        conv_module(first, glu_value, glu_gate, conv_taps, conv_gain, conv_proj),
        1.0,
        second_gain,
    )
    output = post_norm(second, feed_forward(second, last_gate, last_up, last_down), 0.5, third_gain)
    return output[None]


def solution(mesh):
    return jax.shard_map(
        body,
        mesh=mesh,
        in_specs=(
            P("fs", None, "tp"),
            P("fs", "tp"),
            P("fs", "tp"),
            P("tp", "fs"),
            P("tp"),
            P("fs", "tp"),
            P("fs", "tp"),
            P(None, "tp"),
            P("tp"),
            P("tp", "fs"),
            P("tp"),
            P("fs", "tp"),
            P("fs", "tp"),
            P("tp", "fs"),
            P("tp"),
        ),
        out_specs=P("fs", None, "tp"),
        check_vma=False,
    )
```

profile of v0, /device:TPU:0, one launch (start us, length us, event | category | flops | bytes accessed | tf_op | source)
XLA Modules:
  0.0 918.3 jit_solution(3463895856386688371)
XLA Ops:
  6.5 0.7 all-gather.36.cloned.1.call-update
  7.3 0.7 all-gather.14.cloned.1.call-update
  8.1 0.7 all-gather.16.cloned.1.call-update
  8.8 0.5 all-gather.18.cloned.1.call-update
  9.4 21.9 %all-gather.36.cloned.1.call-done = bf16[1,384,2048]{2,1,0:T(8,128)(2,1)} async-done(((bf16[1,384,512]{2,1,0:T(8,128)(2,1)}), bf16[1,384,2048]{2,1,0:T(8,128)(2,1)}) %all-gather.36.cloned.1.call-update) | async-done | bytes 1572880 | tf_op jit(solution)/shard_map/all_gather | solution.py:22
  31.3 100.9 %all-gather.14.cloned.1.call-done = bf16[2048,1536]{1,0:T(8,128)(2,1)} async-done(((bf16[256,1536]{1,0:T(8,128)(2,1)}), bf16[2048,1536]{1,0:T(8,128)(2,1)}) %all-gather.14.cloned.1.call-update) | async-done | bytes 6291472 | tf_op jit(solution)/shard_map/all_gather | solution.py:43
  132.2 7.3 fusion.3
  139.5 91.8 %all-gather.16.cloned.1.call-done = bf16[2048,1536]{1,0:T(8,128)(2,1)} async-done(((bf16[256,1536]{1,0:T(8,128)(2,1)}), bf16[2048,1536]{1,0:T(8,128)(2,1)}) %all-gather.16.cloned.1.call-update) | async-done | bytes 6291472 | tf_op jit(solution)/shard_map/all_gather | solution.py:44
  231.3 99.6 %all-gather.18.cloned.1.call-done = bf16[1536,2048]{1,0:T(8,128)(2,1)} async-done(((bf16[1536,256]{1,0:T(8,128)(2,1)}), bf16[1536,2048]{1,0:T(8,128)(2,1)}) %all-gather.18.cloned.1.call-update) | async-done | bytes 6291472 | tf_op jit(solution)/shard_map/all_gather | solution.py:49
  330.9 11.6 %convolution_convert_fusion.2 = bf16[384,2048]{1,0:T(8,128)(2,1)} fusion(bf16[1536,2048]{1,0:T(8,128)(2,1)} %all-gather.18.cloned.1.call-done, bf16[2048,1536]{1,0:T(8,128)(2,1)} %all-gather.16.cloned.1.call-done, f32[384,1536]{1,0:T(8,128)} %fusion.3, bf16[1,384,2048]{2,1,0:T(8,128)(2,1)S(1)} %copy-done.8), kind=kOutput, calls=%fused_computation.6 | convolution fusion | flops 4836163584 | bytes 18087936 | tf_op jit(solution)/shard_map/dot_general | solution.py:48
  342.5 0.0 all-gather.24.cloned.1.call-start
  342.6 0.5 all-gather.24.cloned.1.call-update
  343.2 25.7 %reduce-scatter.4.cloned.1.call-done = bf16[384,512]{1,0:T(8,128)(2,1)} async-done(((bf16[384,2048]{1,0:T(8,128)(2,1)}), bf16[384,512]{1,0:T(8,128)(2,1)}) %reduce-scatter.4.cloned.1.call-update) | async-done | bytes 393232 | tf_op jit(solution)/shard_map/reduce_scatter | solution.py:26
  368.9 1.3 fusion.12
  370.2 5.8 all-reduce.4
  376.0 2.0 multiply_convert_fusion.2
  378.0 0.0 all-gather.22.cloned.1.call-start
  378.1 0.7 all-gather.22.cloned.1.call-update
  378.8 0.7 all-gather.26.cloned.1.call-update
  379.6 31.6 %all-gather.24.cloned.1.call-done = bf16[2048,256]{1,0:T(8,128)(2,1)} async-done(((bf16[256,256]{1,0:T(8,128)(2,1)}), bf16[2048,256]{1,0:T(8,128)(2,1)}) %all-gather.24.cloned.1.call-update) | async-done | bytes 1048592 | tf_op jit(solution)/shard_map/all_gather | solution.py:60
  411.2 19.9 %all-gather.20.cloned.1.call-done = bf16[384,2048]{1,0:T(8,128)(2,1)} async-done(((bf16[384,512]{1,0:T(8,128)(2,1)}), bf16[384,2048]{1,0:T(8,128)(2,1)}) %all-gather.20.cloned.1.call-update) | async-done | bytes 1572880 | tf_op jit(solution)/shard_map/all_gather | solution.py:22
  431.2 2.4 fusion.7
  433.6 40.0 %all-gather.22.cloned.1.call-done = bf16[2048,256]{1,0:T(8,128)(2,1)} async-done(((bf16[256,256]{1,0:T(8,128)(2,1)}), bf16[2048,256]{1,0:T(8,128)(2,1)}) %all-gather.22.cloned.1.call-update) | async-done | bytes 1048592 | tf_op jit(solution)/shard_map/all_gather | solution.py:59
  473.6 1.8 convolution_multiply_fusion.2
  475.4 1.7 fusion.48
  477.1 5.7 all-reduce.3
  482.8 31.0 %all-gather.26.cloned.1.call-done = bf16[256,2048]{1,0:T(8,128)(2,1)} async-done(((bf16[256,256]{1,0:T(8,128)(2,1)}), bf16[256,2048]{1,0:T(8,128)(2,1)}) %all-gather.26.cloned.1.call-update) | async-done | bytes 1048592 | tf_op jit(solution)/shard_map/all_gather | solution.py:74
  513.8 3.1 convolution_convert_fusion.1
  516.9 0.0 all-gather.30.cloned.1.call-start
  516.9 0.7 all-gather.30.cloned.1.call-update
  517.7 26.4 %reduce-scatter.6.cloned.1.call-done = bf16[384,512]{1,0:T(8,128)(2,1)} async-done(((bf16[384,2048]{1,0:T(8,128)(2,1)}), bf16[384,512]{1,0:T(8,128)(2,1)}) %reduce-scatter.6.cloned.1.call-update) | async-done | bytes 393232 | tf_op jit(solution)/shard_map/reduce_scatter | solution.py:26
  544.1 1.3 fusion.10
  545.4 5.8 all-reduce.2
  551.1 1.9 multiply_convert_fusion.1
  553.1 0.0 all-gather.32.cloned.1.call-start
  553.2 0.7 all-gather.32.cloned.1.call-update
  553.9 0.5 all-gather.34.cloned.1.call-update
  554.4 0.2 reduce-scatter.8.cloned.1.call-start
  554.7 90.3 %all-gather.30.cloned.1.call-done = bf16[2048,1536]{1,0:T(8,128)(2,1)} async-done(((bf16[256,1536]{1,0:T(8,128)(2,1)}), bf16[2048,1536]{1,0:T(8,128)(2,1)}) %all-gather.30.cloned.1.call-update) | async-done | bytes 6291472 | tf_op jit(solution)/shard_map/all_gather | solution.py:43
  645.0 19.3 %all-gather.28.cloned.1.call-done = bf16[384,2048]{1,0:T(8,128)(2,1)} async-done(((bf16[384,512]{1,0:T(8,128)(2,1)}), bf16[384,2048]{1,0:T(8,128)(2,1)}) %all-gather.28.cloned.1.call-update) | async-done | bytes 1572880 | tf_op jit(solution)/shard_map/all_gather | solution.py:22
  664.3 7.4 fusion.51
  671.6 93.5 %all-gather.32.cloned.1.call-done = bf16[2048,1536]{1,0:T(8,128)(2,1)} async-done(((bf16[256,1536]{1,0:T(8,128)(2,1)}), bf16[2048,1536]{1,0:T(8,128)(2,1)}) %all-gather.32.cloned.1.call-update) | async-done | bytes 6291472 | tf_op jit(solution)/shard_map/all_gather | solution.py:44
  765.2 99.6 %all-gather.34.cloned.1.call-done = bf16[1536,2048]{1,0:T(8,128)(2,1)} async-done(((bf16[1536,256]{1,0:T(8,128)(2,1)}), bf16[1536,2048]{1,0:T(8,128)(2,1)}) %all-gather.34.cloned.1.call-update) | async-done | bytes 6291472 | tf_op jit(solution)/shard_map/all_gather | solution.py:49
  864.8 11.6 %convolution_convert_fusion = bf16[384,2048]{1,0:T(8,128)(2,1)} fusion(bf16[1536,2048]{1,0:T(8,128)(2,1)} %all-gather.34.cloned.1.call-done, bf16[384,2048]{1,0:T(8,128)(2,1)S(1)} %copy-done.9, bf16[2048,1536]{1,0:T(8,128)(2,1)} %all-gather.32.cloned.1.call-done, f32[384,1536]{1,0:T(8,128)} %fusion.51), kind=kOutput, calls=%fused_computation.4 | convolution fusion | flops 4836163584 | bytes 18087936 | tf_op jit(solution)/shard_map/dot_general | solution.py:48
  876.4 26.3 %reduce-scatter.8.cloned.1.call-done = bf16[384,512]{1,0:T(8,128)(2,1)} async-done(((bf16[384,2048]{1,0:T(8,128)(2,1)}), bf16[384,512]{1,0:T(8,128)(2,1)}) %reduce-scatter.8.cloned.1.call-update) | async-done | bytes 393232 | tf_op jit(solution)/shard_map/reduce_scatter | solution.py:26
  902.7 1.3 fusion.11
  904.0 5.8 all-reduce.1
  909.8 2.0 fusion.13
  (55 shorter events, 0.7 us)
Async XLA Ops:
  6.5 24.7 %all-gather.36.cloned.1.call-start = ((), (), s32[]{:S(2)}) async-start(), calls=%async_computation.17 | async-start | bytes 1966080 | tf_op jit(solution)/shard_map/all_gather | solution.py:22
  7.3 124.9 %all-gather.14.cloned.1.call-start = ((), (), s32[]{:S(2)}) async-start(), calls=%async_computation.3 | async-start | bytes 7077888 | tf_op jit(solution)/shard_map/all_gather | solution.py:43
  8.0 223.3 %all-gather.16.cloned.1.call-start = ((), (), s32[]{:S(2)}) async-start(), calls=%async_computation.4 | async-start | bytes 7077888 | tf_op jit(solution)/shard_map/all_gather | solution.py:44
  8.7 322.1 %all-gather.18.cloned.1.call-start = ((), (), s32[]{:S(2)}) async-start(), calls=%async_computation.5 | async-start | bytes 7077888 | tf_op jit(solution)/shard_map/all_gather | solution.py:49
  9.3 359.6 %reduce-scatter.4.cloned.1.call-start = ((), (), s32[]{:S(2)}) async-start(), calls=%async_computation.6 | async-start | bytes 1966080 | tf_op jit(solution)/shard_map/reduce_scatter | solution.py:26
  31.3 299.6 %copy-start.8 = (bf16[1,384,2048]{2,1,0:T(8,128)(2,1)S(1)}, bf16[1,384,2048]{2,1,0:T(8,128)(2,1)}, u32[]{:S(2)}) copy-start(bf16[1,384,2048]{2,1,0:T(8,128)(2,1)} %all-gather.36.cloned.1.call-done) | copy-start | bytes 4718596
  139.5 203.7 %copy-start.5 = (bf16[512]{0:T(512)(128)(2,1)S(1)}, bf16[512]{0:T(512)(128)(2,1)}, u32[]{:S(2)}) copy-start(bf16[512]{0:T(512)(128)(2,1)} %param.19) | copy-start | bytes 3076
  139.5 229.5 %copy-start.2 = (bf16[1,384,512]{2,1,0:T(8,128)(2,1)S(1)}, bf16[1,384,512]{2,1,0:T(8,128)(2,1)}, u32[]{:S(2)}) copy-start(bf16[1,384,512]{2,1,0:T(8,128)(2,1)} %param.15) | copy-start | bytes 1179652
  342.5 37.0 %copy-start.10 = (bf16[256]{0:T(256)(128)(2,1)S(1)}, bf16[256]{0:T(256)(128)(2,1)}, u32[]{:S(2)}) copy-start(bf16[256]{0:T(256)(128)(2,1)} %param.23) | copy-start | bytes 1540
  342.5 37.1 %copy-start.4 = (bf16[31,256]{1,0:T(8,128)(2,1)S(1)}, bf16[31,256]{1,0:T(8,128)(2,1)}, u32[]{:S(2)}) copy-start(bf16[31,256]{1,0:T(8,128)(2,1)} %param.22) | copy-start | bytes 47620
  342.5 68.7 %all-gather.24.cloned.1.call-start = ((), (), s32[]{:S(2)}) async-start(), calls=%async_computation.9 | async-start | bytes 1179648 | tf_op jit(solution)/shard_map/all_gather | solution.py:60
  343.1 88.0 %all-gather.20.cloned.1.call-start = ((), (), s32[]{:S(2)}) async-start(), calls=%async_computation.7 | async-start | bytes 1966080 | tf_op jit(solution)/shard_map/all_gather | solution.py:22
  378.0 95.6 %all-gather.22.cloned.1.call-start = ((), (), s32[]{:S(2)}) async-start(), calls=%async_computation.8 | async-start | bytes 1179648 | tf_op jit(solution)/shard_map/all_gather | solution.py:59
  378.8 135.0 %all-gather.26.cloned.1.call-start = ((), (), s32[]{:S(2)}) async-start(), calls=%async_computation.10 | async-start | bytes 1179648 | tf_op jit(solution)/shard_map/all_gather | solution.py:74
  379.5 164.6 %reduce-scatter.6.cloned.1.call-start = ((), (), s32[]{:S(2)}) async-start(), calls=%async_computation.11 | async-start | bytes 1966080 | tf_op jit(solution)/shard_map/reduce_scatter | solution.py:26
  431.2 42.4 %copy-start.3 = (bf16[384,2048]{1,0:T(8,128)(2,1)S(1)}, bf16[384,2048]{1,0:T(8,128)(2,1)}, u32[]{:S(2)}) copy-start(bf16[384,2048]{1,0:T(8,128)(2,1)} %all-gather.20.cloned.1.call-done) | copy-start | bytes 4718596
  513.8 3.9 copy-start.6
  513.8 30.3 %copy-start = (bf16[384,512]{1,0:T(8,128)(2,1)S(1)}, bf16[384,512]{1,0:T(8,128)(2,1)}, u32[]{:S(2)}) copy-start(bf16[384,512]{1,0:T(8,128)(2,1)} %multiply_convert_fusion.2) | copy-start | bytes 1179652
  516.9 128.1 %all-gather.30.cloned.1.call-start = ((), (), s32[]{:S(2)}) async-start(), calls=%async_computation.13 | async-start | bytes 7077888 | tf_op jit(solution)/shard_map/all_gather | solution.py:43
  517.6 146.6 %all-gather.28.cloned.1.call-start = ((), (), s32[]{:S(2)}) async-start(), calls=%async_computation.12 | async-start | bytes 1966080 | tf_op jit(solution)/shard_map/all_gather | solution.py:22
  553.1 212.0 %all-gather.32.cloned.1.call-start = ((), (), s32[]{:S(2)}) async-start(), calls=%async_computation.14 | async-start | bytes 7077888 | tf_op jit(solution)/shard_map/all_gather | solution.py:44
  553.9 310.9 %all-gather.34.cloned.1.call-start = ((), (), s32[]{:S(2)}) async-start(), calls=%async_computation.15 | async-start | bytes 7077888 | tf_op jit(solution)/shard_map/all_gather | solution.py:49
  554.4 348.2 %reduce-scatter.8.cloned.1.call-start = ((), (), s32[]{:S(2)}) async-start(), calls=%async_computation.16 | async-start | bytes 1966080 | tf_op jit(solution)/shard_map/reduce_scatter | solution.py:26
  664.3 200.5 %copy-start.9 = (bf16[384,2048]{1,0:T(8,128)(2,1)S(1)}, bf16[384,2048]{1,0:T(8,128)(2,1)}, u32[]{:S(2)}) copy-start(bf16[384,2048]{1,0:T(8,128)(2,1)} %all-gather.28.cloned.1.call-done) | copy-start | bytes 4718596
  671.6 204.8 %copy-start.7 = (bf16[512]{0:T(512)(128)(2,1)S(1)}, bf16[512]{0:T(512)(128)(2,1)}, u32[]{:S(2)}) copy-start(bf16[512]{0:T(512)(128)(2,1)} %param.29) | copy-start | bytes 3076
  671.6 231.1 %copy-start.1 = (bf16[384,512]{1,0:T(8,128)(2,1)S(1)}, bf16[384,512]{1,0:T(8,128)(2,1)}, u32[]{:S(2)}) copy-start(bf16[384,512]{1,0:T(8,128)(2,1)} %multiply_convert_fusion.1) | copy-start | bytes 1179652
Sparse Core Ops, SparseCore 0:
  8.9 22.3 all-gather.35
  33.5 98.6 all-gather.13
  134.4 96.8 all-gather.15
  233.2 97.6 all-gather.17
  342.7 26.2 reduce-scatter.3
  370.9 40.2 all-gather.23
  412.8 18.3 all-gather.19
  433.3 40.2 all-gather.21
  475.7 38.0 all-gather.25
  517.0 27.0 reduce-scatter.5
  546.3 98.6 all-gather.29
  646.4 17.7 all-gather.27
  666.4 98.6 all-gather.31
  767.1 97.6 all-gather.33
  876.5 26.1 reduce-scatter.7
where the time goes:
time: 919 us; the launch traced here: 918 us
  waiting for transfers between devices  824 us (90%)
  matrix products  45.2 us (5%)
  blocking collectives  23 us (3%)
  between operations  13.5 us (1%)
  other arithmetic  11.5 us (1%)
    all_gather x2, waiting for transfers between devices, feed_forward(): lax.all_gather(w_down, 'fs', axis=1, tiled=True)  199 us
    all_gather x2, waiting for transfers between devices, feed_forward(): lax.all_gather(w_gate, 'fs', axis=0, tiled=True)  191 us
    all_gather x2, waiting for transfers between devices, feed_forward(): lax.all_gather(w_up, 'fs', axis=0, tiled=True)  185 us
    reduce_scatter x3, waiting for transfers between devices, scatter_rows(): lax.psum_scatter(partial_value.astype(jnp.bfloat16), 'tp', scatter_dimens...  78.4 us
    all_gather x3, waiting for transfers between devices, gather_features(): return lax.all_gather(current, 'tp', axis=1, tiled=True)  61.1 us
    all_gather x1, waiting for transfers between devices, conv_module(): lax.all_gather(glu_value, 'fs', axis=0, tiled=True)  40 us
    all_gather x1, waiting for transfers between devices, conv_module(): lax.all_gather(glu_gate, 'fs', axis=0, tiled=True)  31.6 us
    all_gather x1, waiting for transfers between devices, conv_module(): lax.all_gather(conv_proj, 'fs', axis=1, tiled=True)  31 us
  transfers between devices with their start and end apart: 15, of which 15 were waited for; matrix products, arithmetic and copies ran while one was open for 3% of the time, Pallas kernels for 0%

commit v1 on v0

v1 whole, which is shorter than its diff:
```python
import functools

import jax
import jax.numpy as jnp
from jax import lax
from jax.experimental import pallas as pl
from jax.experimental.pallas import tpu as pltpu
from jax.sharding import PartitionSpec as P

ALPHA = 2.0**0.25
EPSILON = 1e-05
MESH = pl.DeviceIdType.MESH
F32 = jnp.float32
BF16 = jnp.bfloat16


def plan_pieces(parts):
    pieces = []
    for matrix, (rows, cuts) in enumerate(parts):
        start = 0
        for size, swapped in cuts(rows):
            pieces.append((matrix, start, size, swapped))
            start += size
    return pieces


def halves(rows):
    return [(rows // 2, False), (rows // 2, False)]


def whole(rows):
    return [(rows, True)]


def half_swapped(rows):
    return [(rows // 2, True), (rows // 2, False)]


def layer_kernel(
    n_fs,
    n_tp,
    n_y,
    pieces,
    tokens_ref,
    *refs,
):
    weights = refs[:9]
    first_gain, conv_taps, conv_gain, second_gain, third_gain = refs[9:14]
    out_ref = refs[14]
    bufs = refs[15:24]
    (xg, rs, send_buf, hidden, current, conv_in, acted, stat, z_s, z_r, y_s, y_r, loc_s, ag_s, ag_r, rs_s, rs_r, st_s, st_r) = refs[24:]

    n_z = n_fs // n_y
    fs = lax.axis_index("fs")
    tp = lax.axis_index("tp")
    z, y = fs // n_y, fs % n_y
    length, width = tokens_ref.shape
    features = width * n_tp

    barrier = pltpu.get_barrier_semaphore()
    for other in range(n_fs):
        @pl.when(other != fs)
        def _():
            pl.semaphore_signal(barrier, inc=1, device_id=(other, tp), device_id_type=MESH)
    for step in range(1, n_tp):
        pl.semaphore_signal(barrier, inc=1, device_id=(fs, (tp + step) % n_tp), device_id_type=MESH)
    pl.semaphore_wait(barrier, n_fs - 1 + n_tp - 1)

    pending = []

    def slot(matrix, start, size, block):
        buf = bufs[matrix]
        if len(buf.shape) == 2:
            rows = weights[matrix].shape[0]
            return buf.at[pl.ds(pl.multiple_of(block * rows + start, 8), size)]
        return buf.at[block, pl.ds(start, size)]

    def remote(src, dst, s, r, dest):
        return pltpu.make_async_remote_copy(
            src_ref=src, dst_ref=dst, send_sem=s, recv_sem=r, device_id=dest, device_id_type=MESH
        )

    def axes(swapped):
        major, minor = (z, n_z, n_y), (y, n_y, 1)
        return (minor, major) if swapped else (major, minor)

    def when(cond, fn):
        pl.when(cond)(fn)

    def place(c, k, d, side):
        _, (_, extent, _) = axes(pieces[c][3])
        return (k * (extent - 1) + d - 1) * 2 + side

    def second_send(c, k, block, src):
        matrix, start, size, swapped = pieces[c]
        _, (pos, extent, stride) = axes(swapped)
        for side, sign in ((0, 1), (1, -1)):
            ok = pos < extent - 1 if side == 0 else pos > 0

            def go(side=side, sign=sign):
                i = place(c, k, 1, side)
                remote(src, slot(matrix, start, size, block), y_s.at[c, i], y_r.at[c, i], (fs + sign * stride, tp)).start()

            def done(side=side, sign=sign):
                i = place(c, k, 1, side)
                remote(src, slot(matrix, start, size, block), y_s.at[c, i], y_r.at[c, i], (fs + sign * stride, tp)).wait_send()

            when(ok, go)
            pending.append((ok, done))

    def own(c):
        matrix, start, size, swapped = pieces[c]
        src = weights[matrix].at[pl.ds(start, size)]
        (pos, extent, stride), _ = axes(swapped)
        for side, sign in ((0, 1), (1, -1)):
            ok = pos < extent - 1 if side == 0 else pos > 0

            def copy(side=side, sign=sign):
                return remote(src, slot(matrix, start, size, fs), z_s.at[c, side], z_r.at[c, side], (fs + sign * stride, tp))

            when(ok, lambda copy=copy: copy().start())
            pending.append((ok, lambda copy=copy: copy().wait_send()))
        second_send(c, 0, fs, src)
        pltpu.make_async_copy(src, slot(matrix, start, size, fs), loc_s.at[c]).start()

    def first_axis(c):
        matrix, start, size, swapped = pieces[c]
        (pos, extent, stride), _ = axes(swapped)
        for d in range(1, extent):
            for side, sign in ((0, 1), (1, -1)):
                here = pos - sign * d >= 0 if side == 0 else pos + d < extent
                onward = here & (pos < extent - 1 if side == 0 else pos > 0)
                block = fs - sign * d * stride
                i = (d - 1) * 2 + side

                def arrive(block=block, i=i):
                    dst = slot(matrix, start, size, block)
                    remote(dst, dst, z_s.at[c, i], z_r.at[c, i], (fs, tp)).wait_recv()

                when(here, arrive)
                if d < extent - 1:
                    def copy(block=block, i=i, sign=sign):
                        dst = slot(matrix, start, size, block)
                        return remote(dst, dst, z_s.at[c, i + 2], z_r.at[c, i + 2], (fs + sign * stride, tp))

                    when(onward, lambda copy=copy: copy().start())
                    pending.append((onward, lambda copy=copy: copy().wait_send()))
                k = 1 + i
                _, (pos2, extent2, stride2) = axes(swapped)
                for side2, sign2 in ((0, 1), (1, -1)):
                    ok = here & (pos2 < extent2 - 1 if side2 == 0 else pos2 > 0)

                    def copy2(block=block, k=k, side2=side2, sign2=sign2, stride2=stride2):
                        j = place(c, k, 1, side2)
                        dst = slot(matrix, start, size, block)
                        return remote(dst, dst, y_s.at[c, j], y_r.at[c, j], (fs + sign2 * stride2, tp))

                    when(ok, lambda copy2=copy2: copy2().start())
                    pending.append((ok, lambda copy2=copy2: copy2().wait_send()))
                yield

    def second_axis(c):
        matrix, start, size, swapped = pieces[c]
        (pos, extent, stride), (pos2, extent2, stride2) = axes(swapped)
        origins = [(0, None, 0)] + [
            (1 + (d - 1) * 2 + side, side, d) for d in range(1, extent) for side in (0, 1)
        ]
        for d2 in range(1, extent2):
            for k, side, d in origins:
                if side is None:
                    here, first = True, fs
                else:
                    sign = 1 if side == 0 else -1
                    here = pos - d >= 0 if side == 0 else pos + d < extent
                    first = fs - sign * d * stride
                for side2, sign2 in ((0, 1), (1, -1)):
                    got = here & (pos2 - d2 >= 0 if side2 == 0 else pos2 + d2 < extent2)
                    block = first - sign2 * d2 * stride2
                    i = place(c, k, d2, side2)

                    def arrive(block=block, i=i):
                        dst = slot(matrix, start, size, block)
                        remote(dst, dst, y_s.at[c, i], y_r.at[c, i], (fs, tp)).wait_recv()

                    when(got, arrive)
                    if d2 < extent2 - 1:
                        ok = got & (pos2 < extent2 - 1 if side2 == 0 else pos2 > 0)

                        def copy(block=block, i=i, sign2=sign2):
                            dst = slot(matrix, start, size, block)
                            return remote(dst, dst, y_s.at[c, i + 2], y_r.at[c, i + 2], (fs + sign2 * stride2, tp))

                        when(ok, lambda copy=copy: copy().start())
                        pending.append((ok, lambda copy=copy: copy().wait_send()))
            yield
        pltpu.make_async_copy(
            weights[matrix].at[pl.ds(start, size)], slot(matrix, start, size, fs), loc_s.at[c]
        ).wait()

    landed = [0]

    def stream():
        count = len(pieces)
        for c in range(min(2, count)):
            own(c)
        yield
        yield from first_axis(0)
        for c in range(count):
            if c + 2 < count:
                own(c + 2)
            if c + 1 < count:
                yield from first_axis(c + 1)
            yield from second_axis(c)
            landed[0] = c + 1
            yield

    pump_state = stream()

    def pump(steps):
        for _ in range(steps):
            next(pump_state, None)

    def until(matrix):
        need = max(i for i, piece in enumerate(pieces) if piece[0] == matrix) + 1
        while landed[0] < need:
            next(pump_state)

    def my_columns():
        return pl.ds(pl.multiple_of(tp * width, 128), width)

    def gather_start(phase, src):
        dst = xg.at[phase, :, my_columns()]
        for step in range(1, n_tp):
            i = step - 1
            remote(src, dst, ag_s.at[phase, i], ag_r.at[phase, i], (fs, (tp + step) % n_tp)).start()

    def gather_wait(phase, src):
        for step in range(1, n_tp):
            i = step - 1
            remote(src, src, ag_s.at[phase, i], ag_r.at[phase, i], (fs, tp)).wait()

    def scatter_start(phase):
        for step in range(1, n_tp):
            i = step - 1
            to = (tp + step) % n_tp
            remote(send_buf.at[to], rs.at[phase, i], rs_s.at[phase, i], rs_r.at[phase, i], (fs, to)).start()

    def scatter_wait(phase):
        for step in range(1, n_tp):
            i = step - 1
            remote(send_buf.at[0], rs.at[phase, i], rs_s.at[phase, i], rs_r.at[phase, i], (fs, tp)).wait()
        total = send_buf[pl.ds(tp, 1)][0].astype(F32)
        for i in range(n_tp - 1):
            total = total + rs[phase, i].astype(F32)
        return total

    def stats_start(phase, values):
        sums = jnp.sum(values, axis=-1, keepdims=True)
        squares = jnp.sum(values * values, axis=-1, keepdims=True)
        lane = lax.broadcasted_iota(jnp.int32, (values.shape[0], 128), 1)
        both = jnp.where(lane == 0, sums, jnp.where(lane == 1, squares, 0.0))
        stat[phase, n_tp - 1] = both.T[:8]
        for step in range(1, n_tp):
            i = step - 1
            remote(
                stat.at[phase, n_tp - 1], stat.at[phase, i], st_s.at[phase, i], st_r.at[phase, i],
                (fs, (tp + step) % n_tp),
            ).start()

    def stats_wait(phase, all_width):
        for step in range(1, n_tp):
            i = step - 1
            remote(
                stat.at[phase, n_tp - 1], stat.at[phase, i], st_s.at[phase, i], st_r.at[phase, i], (fs, tp)
            ).wait()
        total = stat[phase, 0]
        for i in range(1, n_tp):
            total = total + stat[phase, i]
        both = jnp.concatenate([total] * 16, axis=0).T
        center = both[:, 0:1] / all_width
        spread = both[:, 1:2] / all_width - center * center
        return center, lax.rsqrt(spread + EPSILON)

    def ffn_hidden(phase, gate, up):
        tile = min(256, gate.shape[1])

        def step(j, carry):
            cols = pl.ds(pl.multiple_of(j * tile, 128), tile)
            held = xg[phase]
            g = jnp.dot(held, gate[:, cols], preferred_element_type=F32)
            u = jnp.dot(held, up[:, cols], preferred_element_type=F32)
            hidden[:, cols] = (g * jax.nn.sigmoid(g) * u).astype(BF16)
            return carry

        lax.fori_loop(0, gate.shape[1] // tile, step, 0)

    def project(source, buf):
        part = buf.shape[2]
        per = width // part

        def step(t, carry):
            held = source[...]
            for q in range(per):
                send_buf[t, :, q * part : (q + 1) * part] = jnp.dot(
                    held, buf[t * per + q], preferred_element_type=F32
                ).astype(BF16)
            return carry

        lax.fori_loop(0, n_tp, step, 0)

    pump(1)
    xg[0, :, my_columns()] = tokens_ref[...]
    gather_start(0, tokens_ref)
    until(0)
    gather_wait(0, tokens_ref)
    until(1)
    ffn_hidden(0, bufs[0], bufs[1])
    until(2)
    project(hidden, bufs[2])
    scatter_start(0)
    pump(6)
    mixed = ALPHA * tokens_ref[...].astype(F32) + 0.5 * scatter_wait(0)
    current[...] = mixed
    stats_start(0, mixed)
    pump(4)
    center, scale = stats_wait(0, features)
    first = ((current[...] - center) * scale * first_gain[...].astype(F32)).astype(BF16)
    out_ref[...] = first
    xg[1, :, my_columns()] = first
    gather_start(1, out_ref)
    until(4)
    gather_wait(1, out_ref)

    channels = acted.shape[1]
    taps = conv_taps.shape[0]
    reach = (taps - 1) // 2
    margin = (conv_in.shape[0] - length) // 2
    held = xg[1]
    value = jnp.dot(held, bufs[3][...], preferred_element_type=F32)
    gate = jnp.dot(held, bufs[4][...], preferred_element_type=F32)
    conv_in[0:margin] = jnp.zeros((margin, channels), F32)
    conv_in[margin + length :] = jnp.zeros((margin, channels), F32)
    conv_in[margin : margin + length] = value * jax.nn.sigmoid(gate)
    pump(2)
    rows_each = length // 4
    for low in range(0, length, rows_each):
        for left in range(0, channels, 128):
            cols = slice(left, left + 128)
            total = jnp.zeros((rows_each, 128), F32)
            for tap in range(taps):
                start = margin - reach + low + tap
                total = total + conv_taps[tap : tap + 1, cols].astype(F32) * conv_in[start : start + rows_each, cols]
            current[low : low + rows_each, cols] = total
    stats_start(1, current[:, 0:channels])
    pump(4)
    center, scale = stats_wait(1, channels * n_tp)
    normed = (current[:, 0:channels] - center) * scale * conv_gain[...].astype(F32)
    acted[...] = (normed * jax.nn.sigmoid(normed)).astype(BF16)
    until(5)
    project(acted, bufs[5])
    scatter_start(1)
    pump(4)
    mixed = ALPHA * out_ref[...].astype(F32) + scatter_wait(1)
    current[...] = mixed
    stats_start(2, mixed)
    pump(4)
    center, scale = stats_wait(2, features)
    second = ((current[...] - center) * scale * second_gain[...].astype(F32)).astype(BF16)
    out_ref[...] = second
    xg[2, :, my_columns()] = second
    gather_start(2, out_ref)
    pump(4)
    gather_wait(2, out_ref)

    until(7)
    ffn_hidden(2, bufs[6], bufs[7])
    until(8)
    project(hidden, bufs[8])
    scatter_start(2)
    for _ in pump_state:
        pass
    for ok, done in pending:
        when(ok, done)
    mixed = ALPHA * out_ref[...].astype(F32) + 0.5 * scatter_wait(2)
    current[...] = mixed
    stats_start(3, mixed)
    center, scale = stats_wait(3, features)
    out_ref[...] = ((current[...] - center) * scale * third_gain[...].astype(F32)).astype(BF16)


def solution(mesh):
    n_fs, n_tp = mesh.shape["fs"], mesh.shape["tp"]
    n_y = 1 << ((n_fs.bit_length() - 1) // 2)
    if n_fs % n_y:
        n_y = 1

    def body(
        tokens, first_gate, first_up, first_down, first_gain, glu_value, glu_gate, conv_taps, conv_gain,
        conv_proj, second_gain, last_gate, last_up, last_down, third_gain,
    ):
        current = tokens[0]
        length, width = current.shape
        weights = (first_gate, first_up, first_down, glu_value, glu_gate, conv_proj, last_gate, last_up, last_down)
        down = (2, 5, 8)
        cuts = (halves, halves, halves, whole, whole, whole, half_swapped, halves, halves)
        pieces = plan_pieces([(w.shape[0], cut) for w, cut in zip(weights, cuts)])
        n_z = n_fs // n_y
        first_slots = 2 * (max(n_z, n_y) - 1)
        second_slots = 2 * max(
            (1 + 2 * (n_z - 1)) * (n_y - 1),
            (1 + 2 * (n_y - 1)) * (n_z - 1),
        )
        channels = glu_value.shape[1]
        reach = (conv_taps.shape[0] - 1) // 2
        margin = -(-reach // 8) * 8
        bufs = [
            pltpu.VMEM((n_fs,) + w.shape if i in down else (n_fs * w.shape[0], w.shape[1]), BF16)
            for i, w in enumerate(weights)
        ]
        dma = pltpu.SemaphoreType.DMA
        vmem = pl.BlockSpec(memory_space=pltpu.VMEM)
        result = pl.pallas_call(
            functools.partial(layer_kernel, n_fs, n_tp, n_y, pieces),
            out_shape=jax.ShapeDtypeStruct((length, width), BF16),
            in_specs=[vmem] + [pl.BlockSpec(memory_space=pl.ANY)] * 9 + [vmem] * 5,
            out_specs=vmem,
            scratch_shapes=bufs
            + [
                pltpu.VMEM((3, length, width * n_tp), BF16),
                pltpu.VMEM((3, n_tp - 1, length, width), BF16),
                pltpu.VMEM((n_tp, length, width), BF16),
                pltpu.VMEM((length, first_gate.shape[1]), BF16),
                pltpu.VMEM((length, width), F32),
                pltpu.VMEM((length + 2 * margin, channels), F32),
                pltpu.VMEM((length, channels), BF16),
                pltpu.VMEM((4, n_tp, 8, length), F32),
                dma((len(pieces), first_slots)),
                dma((len(pieces), first_slots)),
                dma((len(pieces), second_slots)),
                dma((len(pieces), second_slots)),
                dma((len(pieces),)),
                dma((3, n_tp - 1)),
                dma((3, n_tp - 1)),
                dma((3, n_tp - 1)),
                dma((3, n_tp - 1)),
                dma((4, n_tp - 1)),
                dma((4, n_tp - 1)),
            ],
            compiler_params=pltpu.CompilerParams(
                collective_id=0, has_side_effects=True, vmem_limit_bytes=67000000
            ),
        )(
            current, *weights, first_gain[None], conv_taps, conv_gain[None], second_gain[None], third_gain[None]
        )
        return result[None]

    weight = P("fs", "tp")
    return jax.shard_map(
        body,
        mesh=mesh,
        in_specs=(
            P("fs", None, "tp"), weight, weight, P("tp", "fs"), P("tp"), weight, weight, P(None, "tp"), P("tp"),
            P("tp", "fs"), P("tp"), weight, weight, P("tp", "fs"), P("tp"),
        ),
        out_specs=P("fs", None, "tp"),
        check_vma=False,
    )
```

time: 919 us -> 525 us (0.57)
  waiting for transfers between devices: 824 us -> 0 us
  Pallas kernels: 0 us -> 520 us
  matrix products: 45.2 us -> 0 us
  blocking collectives: 23 us -> 0 us
  between operations: 13.5 us -> 0.02 us
  other arithmetic: 11.5 us -> 0 us
    all_gather x12 -> x0, waiting for transfers between devices: 739 us -> none  [the longest x2 199 us: feed_forward(): lax.all_gather(w_down, 'fs', axis=1, tiled=True)]
    pallas_call x0 -> x1, Pallas kernels: none -> 520 us  [body(): pl.pallas_call(functools.partial(layer_kernel, n_fs, n_tp, n_y, pieces),...]
    reduce_scatter x3 -> x0, waiting for transfers between devices: 78.4 us -> none  [scatter_rows(): lax.psum_scatter(partial_value.astype(jnp.bfloat16), 'tp', scatter_dimens...]
    dot_general x7 -> x0, matrix products: 45.2 us -> none  [the longest x2 23.2 us: feed_forward(): jnp.dot(hidden, lax.all_gather(w_down, 'fs', axis=1, tiled=True), preferr...]
    psum x4 -> x0, blocking collectives: 23 us -> none  [norm_split(): lax.psum((jnp.sum(values, axis=-1, keepdims=True), jnp.sum(values * value...]
  transfers between devices with their start and end apart: 15 -> 0, of which waited for: 15 -> 0; matrix products, arithmetic and copies ran while one was open for 3% -> 0% of each run, Pallas kernels for 0% -> 0%
where the time goes in v1:
time: 525 us
  Pallas kernels  520 us (99%)
    pallas_call x1, Pallas kernels, body(): pl.pallas_call(functools.partial(layer_kernel, n_fs, n_tp, n_y, pieces),...  520 us

profile of v1, /device:TPU:0, one launch (start us, length us, event | category | flops | bytes accessed | tf_op | source)
XLA Modules:
  0.0 525.0 jit_solution(9217283327989547650)
XLA Ops:
  0.0 0.0 copy-start.3
  0.0 0.7 copy-done.3
  0.7 0.0 copy-start
  0.7 0.6 broadcast_in_dim.16.refs_11_
  1.2 0.1 copy-done
  1.3 0.0 copy-start.1
  1.3 0.6 broadcast_in_dim.15.refs_9_
  1.9 0.1 copy-done.1
  2.0 0.0 copy-start.2
  2.0 0.6 broadcast_in_dim.17.refs_12_
  2.6 0.1 copy-done.2
  2.7 0.6 broadcast_in_dim.18.refs_13_
  3.3 519.9 %shard_map.145 = bf16[384,512]{1,0:T(8,128)(2,1)} custom-call(bf16[384,512]{1,0:T(8,128)(2,1)} %bitcast.3, bf16[256,1536]{1,0:T(8,128)(2,1)} %refs_0_.1, bf16[256,1536]{1,0:T(8,128)(2,1)} %refs_1_.1, bf16[1536,256]{1,0:T(8,128)(2,1)} %refs_2_.1, bf16[256,256]{1,0:T(8,128)(2,1)} %refs_3_.1, bf16[256,256]{1,0:T(8,128)(2,1)} %refs_4_.1, ...), custom_call_target="tpu_custom_call" | custom-call | tf_op jit(solution)/shard_map/pallas_call | solution.py:422
  523.2 1.8 copy.17
Async XLA Ops:
  0.0 0.7 copy-start.3
  0.7 0.7 copy-start
  1.3 0.7 copy-start.1
  2.0 0.7 copy-start.2

commit v2 on v1

--- a/solution.py
+++ b/solution.py
@@ -14,26 +14,35 @@
 BF16 = jnp.bfloat16
 
 
-def plan_pieces(parts):
+AHEAD_FIRST = 2
+AHEAD_OWN = 1
+
+
+def split_rows(rows, parts, step=16):
+    swapped = max(step, (rows // 6 + step // 2) // step * step)
+    units = (rows - swapped) // step
+    sizes = [(units * (i + 1) // parts - units * i // parts) * step for i in range(parts)]
+    return sizes, swapped
+
+
+def plan_pieces(shapes, down, small, last):
     pieces = []
-    for matrix, (rows, cuts) in enumerate(parts):
-        start = 0
-        for size, swapped in cuts(rows):
-            pieces.append((matrix, start, size, swapped))
-            start += size
+    for matrix, (rows, columns) in enumerate(shapes):
+        if matrix in small:
+            flip = matrix in down
+            half = rows // 2
+            pieces.append((matrix, 0, half, 0, columns, flip))
+            pieces.append((matrix, half, half, 0, columns, False))
+            continue
+        wide = min(columns, 128) if matrix == last else columns
+        for left in range(0, columns, wide):
+            sizes, swapped = split_rows(rows, 2)
+            order = [(sizes[0], False), (swapped, True)] + [(size, False) for size in sizes[1:]]
+            start = 0
+            for size, flip in order:
+                pieces.append((matrix, start, size, left, wide, flip))
+                start += size
     return pieces
-
-
-def halves(rows):
-    return [(rows // 2, False), (rows // 2, False)]
-
-
-def whole(rows):
-    return [(rows, True)]
-
-
-def half_swapped(rows):
-    return [(rows // 2, True), (rows // 2, False)]
 
 
 def layer_kernel(
@@ -48,7 +57,7 @@
     first_gain, conv_taps, conv_gain, second_gain, third_gain = refs[9:14]
     out_ref = refs[14]
     bufs = refs[15:24]
-    (xg, rs, send_buf, hidden, current, conv_in, acted, stat, z_s, z_r, y_s, y_r, loc_s, ag_s, ag_r, rs_s, rs_r, st_s, st_r) = refs[24:]
+    (xg, rs, send_buf, hidden, current, conv_in, acted, stat, z_s, z_r, y_s, y_r, loc_s, ag_s, ag_r, rs_s, rs_r, st_s, st_r, last_s, last_r) = refs[24:]
 
     n_z = n_fs // n_y
     fs = lax.axis_index("fs")
@@ -68,12 +77,17 @@
 
     pending = []
 
-    def slot(matrix, start, size, block):
+    def slot(c, block):
+        matrix, start, size, left, wide, _ = pieces[c]
         buf = bufs[matrix]
         if len(buf.shape) == 2:
             rows = weights[matrix].shape[0]
-            return buf.at[pl.ds(pl.multiple_of(block * rows + start, 8), size)]
-        return buf.at[block, pl.ds(start, size)]
+            return buf.at[pl.ds(pl.multiple_of(block * rows + start, 16), size)]
+        return buf.at[block, pl.ds(start, size), pl.ds(left, wide)]
+
+    def own_rows(c):
+        matrix, start, size, left, wide, _ = pieces[c]
+        return weights[matrix].at[pl.ds(start, size), pl.ds(left, wide)]
 
     def remote(src, dst, s, r, dest):
         return pltpu.make_async_remote_copy(
@@ -88,43 +102,43 @@
         pl.when(cond)(fn)
 
     def place(c, k, d, side):
-        _, (_, extent, _) = axes(pieces[c][3])
+        _, (_, extent, _) = axes(pieces[c][5])
         return (k * (extent - 1) + d - 1) * 2 + side
 
     def second_send(c, k, block, src):
-        matrix, start, size, swapped = pieces[c]
+        swapped = pieces[c][5]
         _, (pos, extent, stride) = axes(swapped)
         for side, sign in ((0, 1), (1, -1)):
             ok = pos < extent - 1 if side == 0 else pos > 0
 
             def go(side=side, sign=sign):
                 i = place(c, k, 1, side)
-                remote(src, slot(matrix, start, size, block), y_s.at[c, i], y_r.at[c, i], (fs + sign * stride, tp)).start()
+                remote(src, slot(c, block), y_s.at[c, i], y_r.at[c, i], (fs + sign * stride, tp)).start()
 
             def done(side=side, sign=sign):
                 i = place(c, k, 1, side)
-                remote(src, slot(matrix, start, size, block), y_s.at[c, i], y_r.at[c, i], (fs + sign * stride, tp)).wait_send()
+                remote(src, slot(c, block), y_s.at[c, i], y_r.at[c, i], (fs + sign * stride, tp)).wait_send()
 
             when(ok, go)
             pending.append((ok, done))
 
     def own(c):
-        matrix, start, size, swapped = pieces[c]
-        src = weights[matrix].at[pl.ds(start, size)]
+        swapped = pieces[c][5]
+        src = own_rows(c)
         (pos, extent, stride), _ = axes(swapped)
         for side, sign in ((0, 1), (1, -1)):
             ok = pos < extent - 1 if side == 0 else pos > 0
 
             def copy(side=side, sign=sign):
-                return remote(src, slot(matrix, start, size, fs), z_s.at[c, side], z_r.at[c, side], (fs + sign * stride, tp))
+                return remote(src, slot(c, fs), z_s.at[c, side], z_r.at[c, side], (fs + sign * stride, tp))
 
             when(ok, lambda copy=copy: copy().start())
             pending.append((ok, lambda copy=copy: copy().wait_send()))
         second_send(c, 0, fs, src)
-        pltpu.make_async_copy(src, slot(matrix, start, size, fs), loc_s.at[c]).start()
+        pltpu.make_async_copy(src, slot(c, fs), loc_s.at[c]).start()
 
     def first_axis(c):
-        matrix, start, size, swapped = pieces[c]
+        swapped = pieces[c][5]
         (pos, extent, stride), _ = axes(swapped)
         for d in range(1, extent):
             for side, sign in ((0, 1), (1, -1)):
@@ -134,13 +148,13 @@
                 i = (d - 1) * 2 + side
 
                 def arrive(block=block, i=i):
-                    dst = slot(matrix, start, size, block)
+                    dst = slot(c, block)
                     remote(dst, dst, z_s.at[c, i], z_r.at[c, i], (fs, tp)).wait_recv()
 
                 when(here, arrive)
                 if d < extent - 1:
                     def copy(block=block, i=i, sign=sign):
-                        dst = slot(matrix, start, size, block)
+                        dst = slot(c, block)
                         return remote(dst, dst, z_s.at[c, i + 2], z_r.at[c, i + 2], (fs + sign * stride, tp))
 
                     when(onward, lambda copy=copy: copy().start())
@@ -152,7 +166,7 @@
 
                     def copy2(block=block, k=k, side2=side2, sign2=sign2, stride2=stride2):
                         j = place(c, k, 1, side2)
-                        dst = slot(matrix, start, size, block)
+                        dst = slot(c, block)
                         return remote(dst, dst, y_s.at[c, j], y_r.at[c, j], (fs + sign2 * stride2, tp))
 
                     when(ok, lambda copy2=copy2: copy2().start())
@@ -160,7 +174,7 @@
                 yield
 
     def second_axis(c):
-        matrix, start, size, swapped = pieces[c]
+        swapped = pieces[c][5]
         (pos, extent, stride), (pos2, extent2, stride2) = axes(swapped)
         origins = [(0, None, 0)] + [
             (1 + (d - 1) * 2 + side, side, d) for d in range(1, extent) for side in (0, 1)
@@ -179,7 +193,7 @@
                     i = place(c, k, d2, side2)
 
                     def arrive(block=block, i=i):
-                        dst = slot(matrix, start, size, block)
+                        dst = slot(c, block)
                         remote(dst, dst, y_s.at[c, i], y_r.at[c, i], (fs, tp)).wait_recv()
 
                     when(got, arrive)
@@ -187,29 +201,29 @@
                         ok = got & (pos2 < extent2 - 1 if side2 == 0 else pos2 > 0)
 
                         def copy(block=block, i=i, sign2=sign2):
-                            dst = slot(matrix, start, size, block)
+                            dst = slot(c, block)
                             return remote(dst, dst, y_s.at[c, i + 2], y_r.at[c, i + 2], (fs + sign2 * stride2, tp))
 
                         when(ok, lambda copy=copy: copy().start())
                         pending.append((ok, lambda copy=copy: copy().wait_send()))
             yield
-        pltpu.make_async_copy(
-            weights[matrix].at[pl.ds(start, size)], slot(matrix, start, size, fs), loc_s.at[c]
-        ).wait()
+        pltpu.make_async_copy(own_rows(c), slot(c, fs), loc_s.at[c]).wait()
 
     landed = [0]
 
     def stream():
         count = len(pieces)
-        for c in range(min(2, count)):
+        lead = AHEAD_FIRST + AHEAD_OWN
+        for c in range(min(lead, count)):
             own(c)
         yield
-        yield from first_axis(0)
+        for c in range(min(AHEAD_FIRST, count)):
+            yield from first_axis(c)
         for c in range(count):
-            if c + 2 < count:
-                own(c + 2)
-            if c + 1 < count:
-                yield from first_axis(c + 1)
+            if c + lead < count:
+                own(c + lead)
+            if c + AHEAD_FIRST < count:
+                yield from first_axis(c + AHEAD_FIRST)
             yield from second_axis(c)
             landed[0] = c + 1
             yield
@@ -220,8 +234,11 @@
         for _ in range(steps):
             next(pump_state, None)
 
-    def until(matrix):
-        need = max(i for i, piece in enumerate(pieces) if piece[0] == matrix) + 1
+    def until(matrix, right=None):
+        need = 1 + max(
+            i for i, piece in enumerate(pieces)
+            if piece[0] == matrix and (right is None or piece[3] + piece[4] <= right)
+        )
         while landed[0] < need:
             next(pump_state)
 
@@ -245,14 +262,33 @@
             to = (tp + step) % n_tp
             remote(send_buf.at[to], rs.at[phase, i], rs_s.at[phase, i], rs_r.at[phase, i], (fs, to)).start()
 
-    def scatter_wait(phase):
-        for step in range(1, n_tp):
-            i = step - 1
-            remote(send_buf.at[0], rs.at[phase, i], rs_s.at[phase, i], rs_r.at[phase, i], (fs, tp)).wait()
+    def scatter_columns(left, wide, part):
+        copies = []
+        n = left // wide
+        for step in range(1, n_tp):
+            i = step - 1
+            to = (tp + step) % n_tp
+            for q in range(width // part):
+                cols = pl.ds(q * part + left, wide)
+                j = (i * (part // wide) + n) * (width // part) + q
+                copy = remote(
+                    send_buf.at[to, :, cols], rs.at[2, i, :, cols], last_s.at[j], last_r.at[j], (fs, to)
+                )
+                copy.start()
+                copies.append(copy)
+        return copies
+
+    def scatter_total(phase):
         total = send_buf[pl.ds(tp, 1)][0].astype(F32)
         for i in range(n_tp - 1):
             total = total + rs[phase, i].astype(F32)
         return total
+
+    def scatter_wait(phase):
+        for step in range(1, n_tp):
+            i = step - 1
+            remote(send_buf.at[0], rs.at[phase, i], rs_s.at[phase, i], rs_r.at[phase, i], (fs, tp)).wait()
+        return scatter_total(phase)
 
     def stats_start(phase, values):
         sums = jnp.sum(values, axis=-1, keepdims=True)
@@ -294,15 +330,16 @@
 
         lax.fori_loop(0, gate.shape[1] // tile, step, 0)
 
-    def project(source, buf):
+    def project(source, buf, left=0, wide=None):
         part = buf.shape[2]
         per = width // part
+        wide = wide or part
 
         def step(t, carry):
             held = source[...]
             for q in range(per):
-                send_buf[t, :, q * part : (q + 1) * part] = jnp.dot(
-                    held, buf[t * per + q], preferred_element_type=F32
+                send_buf[t, :, q * part + left : q * part + left + wide] = jnp.dot(
+                    held, buf[t * per + q, :, left : left + wide], preferred_element_type=F32
                 ).astype(BF16)
             return carry
 
@@ -374,14 +411,20 @@
 
     until(7)
     ffn_hidden(2, bufs[6], bufs[7])
-    until(8)
-    project(hidden, bufs[8])
-    scatter_start(2)
+    part = bufs[8].shape[2]
+    wide = min(part, 128)
+    copies = []
+    for left in range(0, part, wide):
+        until(8, left + wide)
+        project(hidden, bufs[8], left, wide)
+        copies += scatter_columns(left, wide, part)
     for _ in pump_state:
         pass
     for ok, done in pending:
         when(ok, done)
-    mixed = ALPHA * out_ref[...].astype(F32) + 0.5 * scatter_wait(2)
+    for copy in copies:
+        copy.wait()
+    mixed = ALPHA * out_ref[...].astype(F32) + 0.5 * scatter_total(2)
     current[...] = mixed
     stats_start(3, mixed)
     center, scale = stats_wait(3, features)
@@ -402,8 +445,7 @@
         length, width = current.shape
         weights = (first_gate, first_up, first_down, glu_value, glu_gate, conv_proj, last_gate, last_up, last_down)
         down = (2, 5, 8)
-        cuts = (halves, halves, halves, whole, whole, whole, half_swapped, halves, halves)
-        pieces = plan_pieces([(w.shape[0], cut) for w, cut in zip(weights, cuts)])
+        pieces = plan_pieces([w.shape for w in weights], down, (3, 4, 5), 8)
         n_z = n_fs // n_y
         first_slots = 2 * (max(n_z, n_y) - 1)
         second_slots = 2 * max(
@@ -413,6 +455,7 @@
         channels = glu_value.shape[1]
         reach = (conv_taps.shape[0] - 1) // 2
         margin = -(-reach // 8) * 8
+        n_last = (n_tp - 1) * (width // min(last_down.shape[1], 128))
         bufs = [
             pltpu.VMEM((n_fs,) + w.shape if i in down else (n_fs * w.shape[0], w.shape[1]), BF16)
             for i, w in enumerate(weights)
@@ -445,6 +488,8 @@
                 dma((3, n_tp - 1)),
                 dma((4, n_tp - 1)),
                 dma((4, n_tp - 1)),
+                dma((n_last,)),
+                dma((n_last,)),
             ],
             compiler_params=pltpu.CompilerParams(
                 collective_id=0, has_side_effects=True, vmem_limit_bytes=67000000

time: 525 us -> 444 us (0.85)
  Pallas kernels: 520 us -> 439 us
    pallas_call x1, Pallas kernels: 520 us -> 439 us  [body(): pl.pallas_call(functools.partial(layer_kernel, n_fs, n_tp, n_y, pieces),...]
where the time goes in v2:
time: 444 us
  Pallas kernels  439 us (99%)
  local copies, waits for them, and re-layouts  5.06 us (1%)
    pallas_call x1, Pallas kernels, body(): pl.pallas_call(functools.partial(layer_kernel, n_fs, n_tp, n_y, pieces),...  439 us

profile of v2, /device:TPU:0, one launch (start us, length us, event | category | flops | bytes accessed | tf_op | source)
XLA Modules:
  0.0 443.9 jit_solution(13477865529092632044)
XLA Ops:
  0.0 0.0 copy-start.3
  0.0 0.7 copy-done.3
  0.7 0.0 copy-start
  0.7 0.6 broadcast_in_dim.16.refs_11_
  1.2 0.1 copy-done
  1.3 0.0 copy-start.1
  1.3 0.6 broadcast_in_dim.15.refs_9_
  1.9 0.1 copy-done.1
  2.0 0.0 copy-start.2
  2.0 0.6 broadcast_in_dim.17.refs_12_
  2.6 0.1 copy-done.2
  2.7 0.6 broadcast_in_dim.18.refs_13_
  3.3 438.9 %shard_map.145 = bf16[384,512]{1,0:T(8,128)(2,1)} custom-call(bf16[384,512]{1,0:T(8,128)(2,1)} %bitcast.3, bf16[256,1536]{1,0:T(8,128)(2,1)} %refs_0_.1, bf16[256,1536]{1,0:T(8,128)(2,1)} %refs_1_.1, bf16[1536,256]{1,0:T(8,128)(2,1)} %refs_2_.1, bf16[256,256]{1,0:T(8,128)(2,1)} %refs_3_.1, bf16[256,256]{1,0:T(8,128)(2,1)} %refs_4_.1, ...), custom_call_target="tpu_custom_call" | custom-call | tf_op jit(solution)/shard_map/pallas_call | solution.py:465
  442.2 1.8 copy.17
Async XLA Ops:
  0.0 0.7 copy-start.3
  0.7 0.7 copy-start
  1.3 0.7 copy-start.1
  2.0 0.7 copy-start.2
